TPU v7x, 256 devices: a whole 4x4x8 slice. The times are simulated.
256 devices in a mesh: sp: 32 (over z, y), fs: 4 (over x), tp: 2 (over core).
Axes of the slice: x: 4, y: 4, z: 8, core: 2. Of those that a mesh axis runs over, the one named last changes fastest.
Arguments:
- tokens: bfloat16 [16384, 2048], P(('fs', 'sp'), 'tp'), parts along dimension 0, may hold values from -6 to 6
- norm_gain: float32 [2048], replicated, may hold values from 0.1 to 1.9
- w_recur_in: bfloat16 [2048, 1024], P(None, 'tp'), may hold values from -0.125 to 0.125
- conv_weight: float32 [4, 1024], P(None, 'tp'), may hold values from -3 to 3
- w_gate_decay: bfloat16 [16, 64, 64], P('tp'), may hold values from -0.75 to 0.75
- w_gate_input: bfloat16 [16, 64, 64], P('tp'), may hold values from -0.75 to 0.75
- decay_base: float32 [1024], P('tp'), may hold values from 0 to 0.01, as said below
- extra_decay: float32 [16384, 16], P(('fs', 'sp'), 'tp'), parts along dimension 0, may hold values from 0 to 1, as said below
- w_query: bfloat16 [2048, 1024], P(None, 'tp'), may hold values from -1 to 1
- w_key: bfloat16 [2048, 256], P(None, 'tp'), may hold values from -20 to 20
- w_value: bfloat16 [2048, 256], P(None, 'tp'), may hold values from -0.125 to 0.125
- mix_lambda: float32 [8], P('tp'), may hold values from 0.3 to 0.8
- head_gain: float32 [128], replicated, may hold values from 0.1 to 1.9
- w_out_recur: bfloat16 [1024, 2048], P('tp'), may hold values from -0.125 to 0.125
- w_out_attend: bfloat16 [1024, 2048], P('tp'), may hold values from -0.125 to 0.125
- out_gain: float32 [2048], replicated, may hold values from 0.1 to 1.9
Outputs:
- mixed: bfloat16 [16384, 2048], P(('fs', 'sp', 'tp')), parts along dimension 0
There are 4 independent parts, one for each index of `fs`. A program takes and returns all parts, laid end to end along the dimension named above; an argument that names none is the same for every part. Nothing has to cross between parts.
Inputs may be any that keep to these rules, and one draw needn't show every extreme that they name: `decay_base`: positive rates of each channel. `extra_decay`: non-negative added log-decays.
All inputs are finite; a program needn't handle non-finite values.
Results may differ from a plain program's by a relative error of at most 0.012.
The roundings to bfloat16 on the way count: a program that leaves them out, or rounds other values in their place, can miss the bound.
Values may be sent and summed in bfloat16 or wider, within the bound.
A program may use at most 128 MiB of HBM per device.

v0:
```python
import jax
import jax.numpy as jnp
from jax import lax
from jax.sharding import PartitionSpec as P

D = 2048
HEAD = 64
DV = 128
lru_rate = 8.0
norm_eps = 1e-06


def shifted(block, axis, distance):
    devices = range(lax.axis_size(axis))
    route = [(i - distance, i) for i in devices if i - distance in devices]
    return lax.ppermute(block, axis, route)


def copy_for_each(shard, axis):
    copies = jnp.broadcast_to(shard, (lax.axis_size(axis), *shard.shape))
    return lax.all_to_all(copies, axis, split_axis=0, concat_axis=0, tiled=True)


def all_in_one(shard, axis):
    leaves = jax.tree.leaves(shard)
    sequence = sorted(range(len(leaves)), key=lambda k: -leaves[k].size)
    width = (1, *leaves[sequence[0]].shape)[-1]
    lines = [
        jnp.pad(leaves[k].reshape(-1), (0, -leaves[k].size % width)).reshape(-1, width)
        for k in sequence
    ]
    both, at, found = (copy_for_each(jnp.concatenate(lines), axis), 0, {})
    for k, line in zip(sequence, lines):
        share = both[:, at : at + len(line)].reshape(len(both), -1)
        found[k] = share[:, : leaves[k].size].reshape(-1, *leaves[k].shape)
        at += len(line)
    numbers = iter(range(len(leaves)))
    return jax.tree.map(lambda _: found[next(numbers)], shard)


def folded_in_pairs(pieces, combine):
    while len(jax.tree.leaves(pieces)[0]) > 1:
        pieces = jax.vmap(combine)(
            *(jax.tree.map(lambda part: part[side::2], pieces) for side in (0, 1))
        )
    return jax.tree.map(lambda part: part[0], pieces)


def carried_in(shard, axis, combine, identity):
    length, index = (lax.axis_size(axis), lax.axis_index(axis))
    passed = jnp.arange(length) < index

    def kept(part, zero, own):
        part = jnp.where(
            passed.reshape(-1, *(1 for _ in own.shape)), part, jnp.asarray(zero, own.dtype)
        )
        return part

    pieces = all_in_one(shard, axis)
    return folded_in_pairs(jax.tree.map(kept, pieces, identity, shard), combine)


def in_one_piece(arrays, axis, dim, along):
    both = jnp.concatenate(arrays, axis=along)
    result, at, outs = (lax.all_gather(both, axis, axis=dim, tiled=True), 0, [])
    for a in arrays:
        outs.append(lax.slice_in_dim(result, at, at + a.shape[along], axis=along))
        at += a.shape[along]
    return tuple(outs)


def chain(earlier, later):
    return (earlier[0] * later[0], later[0] * earlier[1] + later[1])


def body(
    tokens,
    norm_gain,
    w_recur_in,
    conv_weight,
    w_gate_decay,
    w_gate_input,
    decay_base,
    extra_decay,
    w_query,
    w_key,
    w_value,
    mix_lambda,
    head_gain,
    w_out_recur,
    w_out_attend,
    out_gain,
):
    row_count = tokens.shape[0]
    recur_cols = w_recur_in.shape[1]
    query_cols = w_query.shape[1]
    key_cols = w_key.shape[1]
    all_weights = jnp.concatenate([w_recur_in, w_query, w_key, w_value], axis=1)
    wide_piece = lax.all_gather(tokens, "tp", axis=1, tiled=True).astype(jnp.float32)
    scaled = (wide_piece * norm_gain).astype(jnp.bfloat16)
    accum = jnp.dot(scaled, all_weights, preferred_element_type=jnp.float32)
    squares = jnp.sum(wide_piece * wide_piece, axis=1, keepdims=True)
    accum, squares = (accum, squares)
    inverse = lax.rsqrt(squares / D + norm_eps)
    projected = (accum * inverse).astype(jnp.bfloat16)
    recur_in = projected[:, :recur_cols]
    queries = projected[:, recur_cols : recur_cols + query_cols]
    keys = projected[:, recur_cols + query_cols : recur_cols + query_cols + key_cols]
    values = projected[:, recur_cols + query_cols + key_cols :]
    taps = conv_weight.shape[0]
    carried_rows = shifted(recur_in[row_count - (taps - 1) :], "sp", 1)
    padded = jnp.concatenate([carried_rows, recur_in], axis=0).astype(jnp.float32)
    conv_acc = jnp.zeros((row_count, recur_cols), jnp.float32)
    for offset in range(taps):
        conv_acc = conv_acc + conv_weight[offset] * padded[offset : offset + row_count]
    conv_in = conv_acc.astype(jnp.bfloat16)
    gate_blocks = w_gate_decay.shape[0]
    blocks = conv_in.reshape(row_count, gate_blocks, HEAD)
    decay_gate = jax.nn.sigmoid(
        jnp.einsum("thi,hij->thj", blocks, w_gate_decay, preferred_element_type=jnp.float32)
    ).reshape(row_count, recur_cols)
    input_gate = jax.nn.sigmoid(
        jnp.einsum("thi,hij->thj", blocks, w_gate_input, preferred_element_type=jnp.float32)
    ).reshape(row_count, recur_cols)
    log_decay = -lru_rate * decay_gate * decay_base - jnp.repeat(extra_decay, HEAD, axis=1)
    decay = jnp.exp(log_decay)
    inject = jnp.sqrt(-jnp.expm1(2.0 * log_decay)) * input_gate * conv_in.astype(jnp.float32)
    decay_cum, local_state = lax.associative_scan(chain, (decay, inject), axis=0)
    identity = (jnp.ones((recur_cols,), jnp.float32), jnp.zeros((recur_cols,), jnp.float32))
    carried = carried_in(
        (decay_cum[row_count - 1], local_state[row_count - 1]), "sp", chain, identity
    )
    recur_out = (local_state + decay_cum * carried[1]).astype(jnp.bfloat16)
    kv_local = key_cols // (2 * HEAD)
    heads_local = query_cols // (2 * HEAD)
    group_size = heads_local // kv_local
    local_query = queries.reshape(row_count, kv_local, group_size, 2, HEAD)
    offset_rows = lax.axis_index("sp") * row_count
    positions = offset_rows + jnp.arange(row_count, dtype=jnp.int32)
    last_position = offset_rows + row_count - 1
    lambdas = mix_lambda.reshape(kv_local, group_size)
    start_state = (
        jnp.full((2, kv_local, group_size, row_count), -1e30, jnp.float32),
        jnp.zeros((2, kv_local, group_size, row_count), jnp.float32),
        jnp.zeros((2, row_count, kv_local, group_size, DV), jnp.float32),
    )
    key_piece, value_piece = in_one_piece((keys, values), "sp", 0, 1)
    count = key_piece.shape[0]

    def update(state):
        peaks, totals, attends = state
        key_three = key_piece.reshape(count, kv_local, 2, HEAD)
        value_three = value_piece.reshape(count, kv_local, DV)
        allowed = positions[:, None] >= jnp.arange(count, dtype=jnp.int32)[None, :]
        new_peaks, new_totals, new_attends = ([], [], [])
        for mapping in range(2):
            scores = jnp.einsum(
                "bkgd,tkd->kgbt",
                local_query[:, :, :, mapping, :],
                key_three[:, :, mapping, :],
                preferred_element_type=jnp.float32,
            ) * HEAD ** (-0.5)
            scores = jnp.where(allowed, scores, -jnp.inf)
            peak = jnp.maximum(peaks[mapping], jnp.max(scores, axis=-1))
            correction = jnp.exp(peaks[mapping] - peak)
            expo = jnp.exp(scores - peak[..., None])
            new_totals.append(totals[mapping] * correction + jnp.sum(expo, axis=-1))
            gained = jnp.einsum(
                "kgbt,tke->bkge",
                expo.astype(jnp.bfloat16),
                value_three,
                preferred_element_type=jnp.float32,
            )
            new_attends.append(
                attends[mapping] * jnp.transpose(correction, (2, 0, 1))[..., None] + gained
            )
            new_peaks.append(peak)
        return (jnp.stack(new_peaks), jnp.stack(new_totals), jnp.stack(new_attends))

    peaks, totals, attends = lax.cond(
        jnp.int32(0) <= last_position, update, lambda state: state, start_state
    )
    first = attends[0] / jnp.transpose(totals[0], (2, 0, 1))[..., None]
    second = attends[1] / jnp.transpose(totals[1], (2, 0, 1))[..., None]
    head_out = (first - lambdas[None, :, :, None] * second).reshape(row_count, heads_local, DV)
    normed = (
        head_out
        * lax.rsqrt(jnp.mean(head_out * head_out, axis=-1, keepdims=True) + norm_eps)
        * head_gain
    )
    attend_out = normed.astype(jnp.bfloat16).reshape(row_count, heads_local * DV)
    recur_rows, attend_rows = (
        lax.all_to_all(recur_out, "tp", split_axis=0, concat_axis=1, tiled=True),
        lax.all_to_all(attend_out, "tp", split_axis=0, concat_axis=1, tiled=True),
    )
    whole_recur, whole_attend = in_one_piece((w_out_recur, w_out_attend), "tp", 0, 1)
    merged = jnp.dot(recur_rows, whole_recur, preferred_element_type=jnp.float32) + jnp.dot(
        attend_rows, whole_attend, preferred_element_type=jnp.float32
    )
    final = (
        merged * lax.rsqrt(jnp.mean(merged * merged, axis=1, keepdims=True) + norm_eps) * out_gain
    )
    return final.astype(jnp.bfloat16)


def solution(mesh):
    in_specs = (
        P(("fs", "sp"), "tp"),
        P(),
        P(None, "tp"),
        P(None, "tp"),
        P("tp", None, None),
        P("tp", None, None),
        P("tp"),
        P(("fs", "sp"), "tp"),
        P(None, "tp"),
        P(None, "tp"),
        P(None, "tp"),
        P("tp"),
        P(),
        P("tp", None),
        P("tp", None),
        P(),
    )
    out_specs = P(("fs", "sp", "tp"), None)
    return jax.shard_map(body, mesh=mesh, in_specs=in_specs, out_specs=out_specs, check_vma=False)
```

profile of v0, /device:TPU:1, one launch (start us, length us, event | category | flops | bytes accessed | tf_op | source)
XLA Modules:
  0.0 134.3 jit_solution(11392075129574978183)
XLA Ops:
  6.5 5.3 %all_gather.9 = bf16[128,2048]{1,0:T(8,128)(2,1)S(1)} all-gather(bf16[128,1024]{1,0:T(8,128)(2,1)} %param.18), channel_id=1, replica_groups=mesh['sp'=32,'fs'=4,'tp'=2] {'tp'}, dimensions={1}, use_global_device_ids=true | all-gather | bytes 786432 | tf_op jit(solution)/shard_map/all_gather | solution.py:99
  12.1 3.3 %fusion.51 = bf16[128,1280]{1,0:T(8,128)(2,1)S(1)} fusion(bf16[2048,128]{1,0:T(8,128)(2,1)} %param.28, bf16[2048,128]{1,0:T(8,128)(2,1)} %param.27, bf16[2048,512]{1,0:T(8,128)(2,1)} %param.26, bf16[2048,512]{1,0:T(8,128)(2,1)} %param.20, bf16[128,2048]{1,0:T(8,128)(2,1)S(1)} %all_gather.9, f32[2048]{0:T(1024)} %param.19, f32[128]{0:T(128)S(1)} %add_rsqrt_fusion.2), kind=kOutput, calls=%fused_computation.54 | convolution fusion | flops 693174272 | bytes 6103552 | tf_op jit(solution)/shard_map/dot_general | solution.py:101
  15.4 0.6 concatenate.68
  16.2 1.6 %collective-permute-start = (bf16[3,512]{1,0:T(4,128)(2,1)S(1)}, bf16[3,512]{1,0:T(4,128)(2,1)S(1)}, u32[]{:S(2)}, u32[]{:S(2)}) collective-permute-start(bf16[3,512]{1,0:T(4,128)(2,1)S(1)} %slice.456), channel_id=1, source_target_pairs={{0,8},{8,16},{16,24},{24,32},{32,40},{40,48},{48,56},{56,64},{64,7... | collective-permute-start | bytes 9224 | tf_op jit(solution)/shard_map/ppermute | solution.py:16
  17.8 4.0 %pad_maximum_fusion.2 = bf16[512,4096]{1,0:T(8,128)(2,1)} fusion(bf16[512,2048]{1,0:T(8,128)(2,1)S(1)} %copy-done.2, bf16[512,2048]{1,0:T(8,128)(2,1)} %param.31), kind=kLoop, calls=%fused_computation.52 | loop fusion | flops 8388608 | bytes 8388608 | tf_op jit(solution)/shard_map/concatenate | solution.py:64
  26.5 0.7 broadcast_in_dim.59
  27.2 10.9 %all-to-all-start = ((f32[32,2,512]{2,1,0:T(2,128)}), f32[32,2,512]{2,1,0:T(2,128)S(1)}, u32[]{:S(2)}, u32[]{:S(2)}) async-start(f32[32,2,512]{2,1,0:T(2,128)} %broadcast_in_dim.59), calls=%async_computation | async-start | bytes 262144 | tf_op jit(solution)/shard_map/all_to_all | solution.py:21
  38.3 9.3 %all-to-all-done = f32[32,2,512]{2,1,0:T(2,128)S(1)} async-done(((f32[32,2,512]{2,1,0:T(2,128)}), f32[32,2,512]{2,1,0:T(2,128)S(1)}, u32[]{:S(2)}, u32[]{:S(2)}) %all-to-all-start) | async-done | bytes 131104 | tf_op jit(solution)/shard_map/all_to_all | solution.py:21
  48.3 5.4 %all_to_all.40 = bf16[2,64,512]{2,1,0:T(8,128)(2,1)S(1)} all-to-all(bf16[2,64,512]{2,1,0:T(8,128)(2,1)S(1)} %bitcast.173), channel_id=1, replica_groups=mesh['sp'=32,'fs'=4,'tp'=2] {'tp'}, dimensions={0} | all-to-all | bytes 262144 | tf_op jit(solution)/shard_map/all_to_all | solution.py:193
  53.7 37.1 %all-gather.5.cloned.1.call-done = bf16[4096,256]{1,0:T(8,128)(2,1)} async-done(((bf16[128,256]{1,0:T(8,128)(2,1)}), bf16[4096,256]{1,0:T(8,128)(2,1)}) %all-gather.5.cloned.1.call-update) | async-done | bytes 2097168 | tf_op jit(solution)/shard_map/all_gather | solution.py:65
  90.8 10.7 %conditional.1 = (f32[2,1,4,128]{3,2,1,0:T(4,128)S(1)}, f32[2,128,1,4,128]{4,1,3,2,0:T(8,128)S(1)}) conditional(s32[]{:T(128)} %convert_element_type.45, () %tuple.13, (s32[]{:T(128)}, s32[128]{0:T(128)S(1)}, bf16[4096,256]{1,0:T(8,128)(2,1)}, bf16[128,1280]{1,0:T(8,128)(2,1)S(1)}) %tuple.14), branch_computations={%region_1.2_spmd, %region_2.7_spmd} | conditional | flops 1640763520 | bytes 70309424 | solution.py:180
  91.1 1.3 slice.238
  92.4 0.5 copy.45
  93.3 1.3 fusion.88
  94.6 1.1 fusion.1
  95.7 1.3 fusion.87
  97.0 1.1 fusion.3
  98.2 1.6 %fusion.21 = f32[1,128,1,4,128]{4,1,3,2,0:T(8,128)S(1)} fusion(f32[1,4,128,4096]{2,3,1,0:T(8,128)S(1)} %get-tuple-element.41, f32[4,128]{1,0:T(4,128)S(1)} %broadcast_maximum_fusion, bf16[4096,256]{1,0:T(8,128)(2,1)S(1)} %copy-done.1, f32[128,4]{0,1:T(4,128)S(1)} %get-tuple-element.45), kind=kOutput, calls=%fused_computation.18 | convolution fusion | flops 541130752 | bytes 9703424 | tf_op jit(solution)/shard_map/cond/branch_1_fun/kgbt,tke->bkge/dot_general | solution.py:168
  99.8 1.6 %fusion.27 = f32[1,128,1,4,128]{4,1,3,2,0:T(8,128)S(1)} fusion(f32[1,4,128,4096]{2,3,1,0:T(8,128)S(1)} %get-tuple-element.43, f32[4,128]{1,0:T(4,128)S(1)} %broadcast_maximum_fusion.1, bf16[4096,256]{1,0:T(8,128)(2,1)S(1)} %copy-done.1, f32[128,4]{0,1:T(4,128)S(1)} %get-tuple-element.36), kind=kOutput, calls=%fused_computation.20 | convolution fusion | flops 541130752 | bytes 9703424 | tf_op jit(solution)/shard_map/cond/branch_1_fun/kgbt,tke->bkge/dot_general | solution.py:168
  103.9 9.0 %all_to_all.41 = bf16[2,64,512]{2,1,0:T(8,128)(2,1)S(1)} all-to-all(bf16[2,64,512]{2,1,0:T(8,128)(2,1)S(1)} %multiply_convert_fusion.1), channel_id=1, replica_groups=mesh['sp'=32,'fs'=4,'tp'=2] {'tp'}, dimensions={0} | all-to-all | bytes 262144 | tf_op jit(solution)/shard_map/all_to_all | solution.py:194
  112.9 7.5 %all-gather.3.cloned.1.call-done = bf16[1024,4096]{1,0:T(8,128)(2,1)} async-done(((bf16[512,4096]{1,0:T(8,128)(2,1)}), bf16[1024,4096]{1,0:T(8,128)(2,1)}) %all-gather.3.cloned.1.call-update) | async-done | bytes 8388624 | tf_op jit(solution)/shard_map/all_gather | solution.py:65
  120.4 3.0 %fusion.44 = f32[64,2048]{1,0:T(8,128)S(1)} fusion(bf16[64,1024]{1,0:T(8,128)(2,1)S(1)} %bitcast.180, bf16[1024,4096]{1,0:T(8,128)(2,1)} %all-gather.3.cloned.1.call-done), kind=kOutput, calls=%fused_computation.48 | convolution fusion | flops 268435456 | bytes 4849664 | tf_op jit(solution)/shard_map/dot_general | solution.py:197
  123.4 3.2 %multiply_reduce_fusion = (f32[64]{0:T(128)S(1)}, f32[64,2048]{1,0:T(8,128)S(1)}) fusion(f32[64,2048]{1,0:T(8,128)S(1)} %fusion.44, bf16[64,1024]{1,0:T(8,128)(2,1)S(1)} %bitcast.172, bf16[1024,4096]{1,0:T(8,128)(2,1)} %all-gather.3.cloned.1.call-done), kind=kOutput, calls=%fused_computation.69 | convolution fusion | flops 268828608 | bytes 5374208 | tf_op jit(solution)/shard_map/dot_general | solution.py:197
  126.6 0.8 multiply_convert_fusion
  (204 shorter events, 8.0 us)
Async XLA Ops:
  6.5 15.8 %copy-start = (bf16[8,64,64]{2,1,0:T(8,128)(2,1)S(1)}, bf16[8,64,64]{2,1,0:T(8,128)(2,1)}, u32[]{:S(2)}) copy-start(bf16[8,64,64]{2,1,0:T(8,128)(2,1)} %param.23) | copy-start | bytes 196612
  6.5 84.3 %all-gather.5.cloned.1.call-start = ((), (), s32[]{:S(2)}) async-start(), calls=%async_computation.4 | async-start | bytes 2162688 | tf_op jit(solution)/shard_map/all_gather | solution.py:65
  12.1 5.7 %copy-start.2 = (bf16[512,2048]{1,0:T(8,128)(2,1)S(1)}, bf16[512,2048]{1,0:T(8,128)(2,1)}, u32[]{:S(2)}) copy-start(bf16[512,2048]{1,0:T(8,128)(2,1)} %param.32) | copy-start | bytes 6291460
  15.4 6.4 %copy-start.4 = (f32[4,512]{1,0:T(4,128)S(1)}, f32[4,512]{1,0:T(4,128)}, u32[]{:S(2)}) copy-start(f32[4,512]{1,0:T(4,128)} %param.21) | copy-start | bytes 24580
  15.4 6.4 %copy-start.7 = (f32[512]{0:T(512)S(1)}, f32[512]{0:T(512)}, u32[]{:S(2)}) copy-start(f32[512]{0:T(512)} %param.24) | copy-start | bytes 6148
  15.4 6.4 %copy-start.5 = (f32[128,8]{0,1:T(8,128)S(1)}, f32[128,8]{0,1:T(8,128)}, u32[]{:S(2)}) copy-start(f32[128,8]{0,1:T(8,128)} %param.25) | copy-start | bytes 12292
  16.1 104.3 %all-gather.3.cloned.1.call-start = ((), (), s32[]{:S(2)}) async-start(), calls=%async_computation.3 | async-start | bytes 12582912 | tf_op jit(solution)/shard_map/all_gather | solution.py:65
  16.2 6.6 %copy-start.9 = (bf16[8,64,64]{2,1,0:T(8,128)(2,1)S(1)}, bf16[8,64,64]{2,1,0:T(8,128)(2,1)}, u32[]{:S(2)}) copy-start(bf16[8,64,64]{2,1,0:T(8,128)(2,1)} %param.22) | copy-start | bytes 196612
  16.2 5.9 %collective-permute-start = (bf16[3,512]{1,0:T(4,128)(2,1)S(1)}, bf16[3,512]{1,0:T(4,128)(2,1)S(1)}, u32[]{:S(2)}, u32[]{:S(2)}) collective-permute-start(bf16[3,512]{1,0:T(4,128)(2,1)S(1)} %slice.456), channel_id=1, source_target_pairs={{0,8},{8,16},{16,24},{24,32},{32,40},{40,48},{48,56},{56,64},{64,7... | collective-permute-start | bytes 9224 | tf_op jit(solution)/shard_map/ppermute | solution.py:16
  22.8 15.4 %copy-start.6 = (f32[4]{0:T(128)S(1)}, f32[4]{0:T(128)}, u32[]{:S(2)}) copy-start(f32[4]{0:T(128)} %param.29) | copy-start | bytes 52
  22.8 15.4 %copy-start.8 = (f32[128]{0:T(128)S(1)}, f32[128]{0:T(128)}, u32[]{:S(2)}) copy-start(f32[128]{0:T(128)} %param.30) | copy-start | bytes 1540
  27.2 20.4 %all-to-all-start = ((f32[32,2,512]{2,1,0:T(2,128)}), f32[32,2,512]{2,1,0:T(2,128)S(1)}, u32[]{:S(2)}, u32[]{:S(2)}) async-start(f32[32,2,512]{2,1,0:T(2,128)} %broadcast_in_dim.59), calls=%async_computation | async-start | bytes 262144 | tf_op jit(solution)/shard_map/all_to_all | solution.py:21
  95.7 2.5 %copy-start.1 = (bf16[4096,256]{1,0:T(8,128)(2,1)S(1)}, bf16[4096,256]{1,0:T(8,128)(2,1)}, u32[]{:S(2)}) copy-start(bf16[4096,256]{1,0:T(8,128)(2,1)} %get-tuple-element.22) | copy-start | bytes 6291460 | tf_op jit(solution)/shard_map/cond
  102.5 24.1 %copy-start.3 = (f32[2048]{0:T(1024)S(1)}, f32[2048]{0:T(1024)}, u32[]{:S(2)}) copy-start(f32[2048]{0:T(1024)} %param.33) | copy-start | bytes 24580
Sparse Core Ops, SparseCore 0:
  16.2 74.5 all-gather.4
  92.6 27.7 all-gather.2
where the time goes:
time: 135 us; the launch traced here: 134 us
  waiting for transfers between devices  54 us (40%)
  blocking collectives  19.7 us (15%)
  matrix products  15.9 us (12%)
  between operations  14.4 us (11%)
  starting transfers between devices  12.6 us (9%)
  other arithmetic  9.36 us (7%)
  local copies, waits for them, and re-layouts  8.21 us (6%)
    all_gather x2, waiting for transfers between devices, in_one_piece(): result, at, outs = (lax.all_gather(both, axis, axis=dim, tiled=True), 0, [])  44.6 us
    all_to_all x1, starting transfers between devices, copy_for_each(): return lax.all_to_all(copies, axis, split_axis=0, concat_axis=0, tiled=True)  10.9 us
    all_to_all x1, waiting for transfers between devices, copy_for_each(): return lax.all_to_all(copies, axis, split_axis=0, concat_axis=0, tiled=True)  9.34 us
    all_to_all x1, blocking collectives, body(): lax.all_to_all(attend_out, 'tp', split_axis=0, concat_axis=1, tiled=True)  8.96 us
    all_to_all x1, blocking collectives, body(): lax.all_to_all(recur_out, 'tp', split_axis=0, concat_axis=1, tiled=True)  5.39 us
    all_gather x1, blocking collectives, body(): lax.all_gather(tokens, 'tp', axis=1, tiled=True).astype(jnp.float32)  5.34 us
    concatenate x1, other arithmetic, in_one_piece(): both = jnp.concatenate(arrays, axis=along)  3.96 us
    dot_general x1, matrix products, body(): accum = jnp.dot(scaled, all_weights, preferred_element_type=jnp.float32)  3.32 us
  transfers between devices with their start and end apart: 4, of which 3 were waited for; matrix products, arithmetic and copies ran while one was open for 17% of the time, Pallas kernels for 0%

commit v1 on v0

--- a/solution.py
+++ b/solution.py
@@ -2,6 +2,7 @@
 import jax.numpy as jnp
 from jax import lax
 from jax.sharding import PartitionSpec as P
+from jax.lax import all_to_all, psum
 
 D = 2048
 HEAD = 64
@@ -96,7 +97,9 @@
     query_cols = w_query.shape[1]
     key_cols = w_key.shape[1]
     all_weights = jnp.concatenate([w_recur_in, w_query, w_key, w_value], axis=1)
-    wide_piece = lax.all_gather(tokens, "tp", axis=1, tiled=True).astype(jnp.float32)
+    wide_piece = jnp.concatenate(
+        all_to_all(jnp.stack([tokens for _ in range(psum(1, "tp"))]), "tp", 0, 0), axis=1
+    ).astype(jnp.float32)
     scaled = (wide_piece * norm_gain).astype(jnp.bfloat16)
     accum = jnp.dot(scaled, all_weights, preferred_element_type=jnp.float32)
     squares = jnp.sum(wide_piece * wide_piece, axis=1, keepdims=True)

time: 135 us -> 139 us (1.030)
  blocking collectives: 19.7 us -> 21.3 us
    all_to_all x0 -> x1, blocking collectives: none -> 6.98 us  [body(): all_to_all(jnp.stack([tokens for _ in range(psum(1, 'tp'))]), 'tp', 0, 0)]
    all_gather x1 -> x0, blocking collectives: 5.34 us -> none  [body(): lax.all_gather(tokens, 'tp', axis=1, tiled=True).astype(jnp.float32)]
  transfers between devices with their start and end apart: 4 -> 4, of which waited for: 3 -> 3; matrix products, arithmetic and copies ran while one was open for 17% -> 16% of each run, Pallas kernels for 0% -> 0%
where the time goes in v1:
time: 139 us; the launch traced here: 138 us
  waiting for transfers between devices  54 us (39%)
  blocking collectives  21.3 us (15%)
  matrix products  15.9 us (11%)
  between operations  14.5 us (10%)
  starting transfers between devices  12.6 us (9%)
  other arithmetic  10.5 us (8%)
  local copies, waits for them, and re-layouts  9.37 us (7%)
    all_gather x2, waiting for transfers between devices, in_one_piece(): result, at, outs = (lax.all_gather(both, axis, axis=dim, tiled=True), 0, [])  44.6 us
    all_to_all x1, starting transfers between devices, copy_for_each(): return lax.all_to_all(copies, axis, split_axis=0, concat_axis=0, tiled=True)  10.9 us
    all_to_all x1, waiting for transfers between devices, copy_for_each(): return lax.all_to_all(copies, axis, split_axis=0, concat_axis=0, tiled=True)  9.28 us
    all_to_all x1, blocking collectives, body(): lax.all_to_all(attend_out, 'tp', split_axis=0, concat_axis=1, tiled=True)  8.96 us
    all_to_all x1, blocking collectives, body(): all_to_all(jnp.stack([tokens for _ in range(psum(1, 'tp'))]), 'tp', 0, 0)  6.98 us
    all_to_all x1, blocking collectives, body(): lax.all_to_all(recur_out, 'tp', split_axis=0, concat_axis=1, tiled=True)  5.4 us
    concatenate x1, other arithmetic, in_one_piece(): both = jnp.concatenate(arrays, axis=along)  3.96 us
    dot_general x1, matrix products, body(): accum = jnp.dot(scaled, all_weights, preferred_element_type=jnp.float32)  3.31 us
  transfers between devices with their start and end apart: 4, of which 3 were waited for; matrix products, arithmetic and copies ran while one was open for 16% of the time, Pallas kernels for 0%

profile of v1, /device:TPU:1, one launch (start us, length us, event | category | flops | bytes accessed | tf_op | source)
XLA Modules:
  0.0 138.3 jit_solution(9746811293464727093)
XLA Ops:
  6.5 1.2 copy.51
  7.7 7.0 %all_to_all.45 = bf16[2,128,1024]{1,2,0:T(8,128)(2,1)S(1)} all-to-all(bf16[2,128,1024]{1,2,0:T(8,128)(2,1)S(1)} %pad_maximum_fusion.3), channel_id=1, replica_groups=mesh['sp'=32,'fs'=4,'tp'=2] {'tp'}, dimensions={0} | all-to-all | bytes 1048576 | tf_op jit(solution)/shard_map/all_to_all | solution.py:101
  15.0 1.0 fusion.63
  16.1 3.3 %fusion.51 = bf16[128,1280]{1,0:T(8,128)(2,1)S(1)} fusion(bf16[128,2048]{0,1:T(8,128)(2,1)S(1)} %fusion.63, bf16[2048,128]{1,0:T(8,128)(2,1)} %param.28, bf16[2048,128]{1,0:T(8,128)(2,1)} %param.27, bf16[2048,512]{1,0:T(8,128)(2,1)} %param.26, bf16[2048,512]{1,0:T(8,128)(2,1)} %param.20, f32[128]{0:T(128)S(1)} %add_rsqrt_fusion.2), kind=kOutput, calls=%fused_computation.54 | convolution fusion | flops 692387840 | bytes 6095360 | tf_op jit(solution)/shard_map/dot_general | solution.py:104
  20.1 1.6 %collective-permute-start = (bf16[3,512]{1,0:T(4,128)(2,1)S(1)}, bf16[3,512]{1,0:T(4,128)(2,1)S(1)}, u32[]{:S(2)}, u32[]{:S(2)}) collective-permute-start(bf16[3,512]{1,0:T(4,128)(2,1)S(1)} %slice.456), channel_id=1, source_target_pairs={{0,8},{8,16},{16,24},{24,32},{32,40},{40,48},{48,56},{56,64},{64,7... | collective-permute-start | bytes 9224 | tf_op jit(solution)/shard_map/ppermute | solution.py:17
  21.8 4.0 %pad_maximum_fusion.2 = bf16[512,4096]{1,0:T(8,128)(2,1)} fusion(bf16[512,2048]{1,0:T(8,128)(2,1)S(1)} %copy-done.2, bf16[512,2048]{1,0:T(8,128)(2,1)} %param.31), kind=kLoop, calls=%fused_computation.52 | loop fusion | flops 8388608 | bytes 8388608 | tf_op jit(solution)/shard_map/concatenate | solution.py:65
  30.5 0.7 broadcast_in_dim.59
  31.2 10.9 %all-to-all-start.1 = ((f32[32,2,512]{2,1,0:T(2,128)}), f32[32,2,512]{2,1,0:T(2,128)S(1)}, u32[]{:S(2)}, u32[]{:S(2)}) async-start(f32[32,2,512]{2,1,0:T(2,128)} %broadcast_in_dim.59), calls=%async_computation.1 | async-start | bytes 262144 | tf_op jit(solution)/shard_map/all_to_all | solution.py:22
  42.2 9.3 %all-to-all-done.1 = f32[32,2,512]{2,1,0:T(2,128)S(1)} async-done(((f32[32,2,512]{2,1,0:T(2,128)}), f32[32,2,512]{2,1,0:T(2,128)S(1)}, u32[]{:S(2)}, u32[]{:S(2)}) %all-to-all-start.1) | async-done | bytes 131104 | tf_op jit(solution)/shard_map/all_to_all | solution.py:22
  52.2 5.4 %all_to_all.46 = bf16[2,64,512]{2,1,0:T(8,128)(2,1)S(1)} all-to-all(bf16[2,64,512]{2,1,0:T(8,128)(2,1)S(1)} %bitcast.182), channel_id=1, replica_groups=mesh['sp'=32,'fs'=4,'tp'=2] {'tp'}, dimensions={0} | all-to-all | bytes 262144 | tf_op jit(solution)/shard_map/all_to_all | solution.py:196
  57.6 37.2 %all-gather.5.cloned.1.call-done = bf16[4096,256]{1,0:T(8,128)(2,1)} async-done(((bf16[128,256]{1,0:T(8,128)(2,1)}), bf16[4096,256]{1,0:T(8,128)(2,1)}) %all-gather.5.cloned.1.call-update) | async-done | bytes 2097168 | tf_op jit(solution)/shard_map/all_gather | solution.py:66
  94.8 10.7 %conditional.1 = (f32[2,1,4,128]{3,2,1,0:T(4,128)S(1)}, f32[2,128,1,4,128]{4,1,3,2,0:T(8,128)S(1)}) conditional(s32[]{:T(128)} %convert_element_type.58, () %tuple.13, (s32[]{:T(128)}, s32[128]{0:T(128)S(1)}, bf16[4096,256]{1,0:T(8,128)(2,1)}, bf16[128,1280]{1,0:T(8,128)(2,1)S(1)}) %tuple.14), branch_computations={%region_1.2_spmd, %region_2.7_spmd} | conditional | flops 1640763520 | bytes 70309424 | solution.py:183
  95.0 1.3 slice.238
  97.2 1.3 fusion.85
  98.5 1.1 fusion.1
  99.7 1.3 fusion.84
  101.0 1.1 fusion.3
  102.2 1.6 %fusion.21 = f32[1,128,1,4,128]{4,1,3,2,0:T(8,128)S(1)} fusion(f32[1,4,128,4096]{2,3,1,0:T(8,128)S(1)} %get-tuple-element.41, f32[4,128]{1,0:T(4,128)S(1)} %broadcast_maximum_fusion, bf16[4096,256]{1,0:T(8,128)(2,1)S(1)} %copy-done.1, f32[128,4]{0,1:T(4,128)S(1)} %get-tuple-element.45), kind=kOutput, calls=%fused_computation.18 | convolution fusion | flops 541130752 | bytes 9703424 | tf_op jit(solution)/shard_map/cond/branch_1_fun/kgbt,tke->bkge/dot_general | solution.py:171
  103.8 1.6 %fusion.27 = f32[1,128,1,4,128]{4,1,3,2,0:T(8,128)S(1)} fusion(f32[1,4,128,4096]{2,3,1,0:T(8,128)S(1)} %get-tuple-element.43, f32[4,128]{1,0:T(4,128)S(1)} %broadcast_maximum_fusion.1, bf16[4096,256]{1,0:T(8,128)(2,1)S(1)} %copy-done.1, f32[128,4]{0,1:T(4,128)S(1)} %get-tuple-element.36), kind=kOutput, calls=%fused_computation.20 | convolution fusion | flops 541130752 | bytes 9703424 | tf_op jit(solution)/shard_map/cond/branch_1_fun/kgbt,tke->bkge/dot_general | solution.py:171
  107.9 9.0 %all_to_all.47 = bf16[2,64,512]{2,1,0:T(8,128)(2,1)S(1)} all-to-all(bf16[2,64,512]{2,1,0:T(8,128)(2,1)S(1)} %multiply_convert_fusion.1), channel_id=1, replica_groups=mesh['sp'=32,'fs'=4,'tp'=2] {'tp'}, dimensions={0} | all-to-all | bytes 262144 | tf_op jit(solution)/shard_map/all_to_all | solution.py:197
  116.9 7.5 %all-gather.3.cloned.1.call-done = bf16[1024,4096]{1,0:T(8,128)(2,1)} async-done(((bf16[512,4096]{1,0:T(8,128)(2,1)}), bf16[1024,4096]{1,0:T(8,128)(2,1)}) %all-gather.3.cloned.1.call-update) | async-done | bytes 8388624 | tf_op jit(solution)/shard_map/all_gather | solution.py:66
  124.4 3.0 %fusion.44 = f32[64,2048]{1,0:T(8,128)S(1)} fusion(bf16[64,1024]{1,0:T(8,128)(2,1)S(1)} %bitcast.189, bf16[1024,4096]{1,0:T(8,128)(2,1)} %all-gather.3.cloned.1.call-done), kind=kOutput, calls=%fused_computation.48 | convolution fusion | flops 268435456 | bytes 4849664 | tf_op jit(solution)/shard_map/dot_general | solution.py:200
  127.4 3.2 %multiply_reduce_fusion.1 = (f32[64]{0:T(128)S(1)}, f32[64,2048]{1,0:T(8,128)S(1)}) fusion(f32[64,2048]{1,0:T(8,128)S(1)} %fusion.44, bf16[64,1024]{1,0:T(8,128)(2,1)S(1)} %bitcast.181, bf16[1024,4096]{1,0:T(8,128)(2,1)} %all-gather.3.cloned.1.call-done), kind=kOutput, calls=%fused_computation.69 | convolution fusion | flops 268828608 | bytes 5374208 | tf_op jit(solution)/shard_map/dot_general | solution.py:200
  130.6 0.8 multiply_convert_fusion
  (207 shorter events, 9.3 us)
Async XLA Ops:
  6.5 19.8 %copy-start = (bf16[8,64,64]{2,1,0:T(8,128)(2,1)S(1)}, bf16[8,64,64]{2,1,0:T(8,128)(2,1)}, u32[]{:S(2)}) copy-start(bf16[8,64,64]{2,1,0:T(8,128)(2,1)} %param.23) | copy-start | bytes 196612
  6.5 88.3 %all-gather.5.cloned.1.call-start = ((), (), s32[]{:S(2)}) async-start(), calls=%async_computation.5 | async-start | bytes 2162688 | tf_op jit(solution)/shard_map/all_gather | solution.py:66
  16.1 5.7 %copy-start.2 = (bf16[512,2048]{1,0:T(8,128)(2,1)S(1)}, bf16[512,2048]{1,0:T(8,128)(2,1)}, u32[]{:S(2)}) copy-start(bf16[512,2048]{1,0:T(8,128)(2,1)} %param.32) | copy-start | bytes 6291460
  19.4 6.4 %copy-start.4 = (f32[4,512]{1,0:T(4,128)S(1)}, f32[4,512]{1,0:T(4,128)}, u32[]{:S(2)}) copy-start(f32[4,512]{1,0:T(4,128)} %param.21) | copy-start | bytes 24580
  19.4 6.4 %copy-start.7 = (f32[512]{0:T(512)S(1)}, f32[512]{0:T(512)}, u32[]{:S(2)}) copy-start(f32[512]{0:T(512)} %param.24) | copy-start | bytes 6148
  19.4 6.4 %copy-start.5 = (f32[128,8]{0,1:T(8,128)S(1)}, f32[128,8]{0,1:T(8,128)}, u32[]{:S(2)}) copy-start(f32[128,8]{0,1:T(8,128)} %param.25) | copy-start | bytes 12292
  20.1 104.3 %all-gather.3.cloned.1.call-start = ((), (), s32[]{:S(2)}) async-start(), calls=%async_computation.4 | async-start | bytes 12582912 | tf_op jit(solution)/shard_map/all_gather | solution.py:66
  20.1 6.6 %copy-start.9 = (bf16[8,64,64]{2,1,0:T(8,128)(2,1)S(1)}, bf16[8,64,64]{2,1,0:T(8,128)(2,1)}, u32[]{:S(2)}) copy-start(bf16[8,64,64]{2,1,0:T(8,128)(2,1)} %param.22) | copy-start | bytes 196612
  20.1 5.9 %collective-permute-start = (bf16[3,512]{1,0:T(4,128)(2,1)S(1)}, bf16[3,512]{1,0:T(4,128)(2,1)S(1)}, u32[]{:S(2)}, u32[]{:S(2)}) collective-permute-start(bf16[3,512]{1,0:T(4,128)(2,1)S(1)} %slice.456), channel_id=1, source_target_pairs={{0,8},{8,16},{16,24},{24,32},{32,40},{40,48},{48,56},{56,64},{64,7... | collective-permute-start | bytes 9224 | tf_op jit(solution)/shard_map/ppermute | solution.py:17
  26.8 15.4 %copy-start.6 = (f32[4]{0:T(128)S(1)}, f32[4]{0:T(128)}, u32[]{:S(2)}) copy-start(f32[4]{0:T(128)} %param.29) | copy-start | bytes 52
  26.8 15.4 %copy-start.8 = (f32[128]{0:T(128)S(1)}, f32[128]{0:T(128)}, u32[]{:S(2)}) copy-start(f32[128]{0:T(128)} %param.30) | copy-start | bytes 1540
  31.2 20.3 %all-to-all-start.1 = ((f32[32,2,512]{2,1,0:T(2,128)}), f32[32,2,512]{2,1,0:T(2,128)S(1)}, u32[]{:S(2)}, u32[]{:S(2)}) async-start(f32[32,2,512]{2,1,0:T(2,128)} %broadcast_in_dim.59), calls=%async_computation.1 | async-start | bytes 262144 | tf_op jit(solution)/shard_map/all_to_all | solution.py:22
  99.7 2.5 %copy-start.1 = (bf16[4096,256]{1,0:T(8,128)(2,1)S(1)}, bf16[4096,256]{1,0:T(8,128)(2,1)}, u32[]{:S(2)}) copy-start(bf16[4096,256]{1,0:T(8,128)(2,1)} %get-tuple-element.22) | copy-start | bytes 6291460 | tf_op jit(solution)/shard_map/cond
  106.5 24.1 %copy-start.3 = (f32[2048]{0:T(1024)S(1)}, f32[2048]{0:T(1024)}, u32[]{:S(2)}) copy-start(f32[2048]{0:T(1024)} %param.33) | copy-start | bytes 24580
Sparse Core Ops, SparseCore 0:
  20.2 74.5 all-gather.4
  96.6 27.7 all-gather.2
